TPU v7x, 32 devices: a whole 2x2x4 slice. The times are simulated.
32 devices in a mesh: sp: 8 (over z, y), tp: 4 (over x, core).
Axes of the slice: x: 2, y: 2, z: 4, core: 2. Of those that a mesh axis runs over, the one named last changes fastest.
Arguments:
- queries_nope: bfloat16 [3072, 8, 128], P('sp', 'tp'), may hold values from -9 to 9
- queries_rope: bfloat16 [3072, 8, 64], P('sp', 'tp'), may hold values from -6 to 6
- latent: bfloat16 [3072, 512], P('sp'), may hold values from -8 to 8, as said below
- rope_key: bfloat16 [3072, 64], P('sp'), may hold values from -6 to 6
- latent_gain: float32 [512], replicated, may hold values from 0.1 to 1.9
- key_up: bfloat16 [512, 1024], P(None, 'tp'), may hold values from -0.25 to 0.25
- value_up: bfloat16 [512, 1024], P(None, 'tp'), may hold values from -0.25 to 0.25
- out_proj: bfloat16 [1024, 2048], P('tp'), may hold values from -0.75 to 0.75
- stream: bfloat16 [3072, 2048], P(('sp', 'tp')), may hold values from -6 to 6
- mix_gain: float32 [2048], replicated, may hold values from 0.1 to 1.9
- w_gate: bfloat16 [2048, 3072], P('sp', 'tp'), may hold values from -0.125 to 0.125
- w_up: bfloat16 [2048, 3072], P('sp', 'tp'), may hold values from -0.125 to 0.125
- w_down: bfloat16 [3072, 2048], P('tp', 'sp'), may hold values from -0.4375 to 0.4375
- mlp_gain: float32 [2048], replicated, may hold values from 0.1 to 1.9
Outputs:
- result: bfloat16 [3072, 2048], P(('sp', 'tp'))
Inputs may be any that keep to these rules, and one draw needn't show every extreme that they name: latent rows carry a mean vector that changes from one eighth of the sequence to the next.
All inputs are finite; a program needn't handle non-finite values.
Results may differ from a plain program's by a relative error of at most 0.017.
Values may be sent and summed in bfloat16 or wider, within the bound.
A program may use at most 192 MiB of HBM per device.

v0:
```python
import jax
import jax.numpy as jnp
from jax import lax
from jax.sharding import PartitionSpec as P

theta_base = 10000.0
residual_weight = 8.0**0.25
norm_floor = 1.0
big_negative = -1e30


def rotate(vector, first_row):
    half = vector.shape[-1] // 2
    rates = theta_base ** (-2.0 * jnp.arange(half, dtype=jnp.float32) / vector.shape[-1])
    places = (first_row + jnp.arange(vector.shape[0], dtype=jnp.int32)).astype(jnp.float32)
    angle = places[:, None] * rates[None, :]
    angle = angle.reshape((vector.shape[0],) + (1,) * (vector.ndim - 2) + (half,))
    cosine = jnp.cos(angle)
    sine = jnp.sin(angle)
    left = vector[..., :half]
    right = vector[..., half:]
    return jnp.concatenate([left * cosine - right * sine, left * sine + right * cosine], axis=-1)


def latent_norm(latent, latent_gain):
    wide = latent.astype(jnp.float32)
    factor = lax.rsqrt(jnp.mean(wide * wide, axis=-1, keepdims=True) + norm_floor)
    return (wide * factor * latent_gain).astype(jnp.bfloat16)


def layer_norm(values, gain):
    centre = jnp.mean(values, axis=-1, keepdims=True)
    centred = values - centre
    spread = jnp.mean(centred * centred, axis=-1, keepdims=True)
    return centred * lax.rsqrt(spread + norm_floor) * gain


def per_device(
    queries_nope,
    queries_rope,
    latent,
    rope_key,
    latent_gain,
    key_up,
    value_up,
    out_proj,
    stream,
    mix_gain,
    w_gate,
    w_up,
    w_down,
    mlp_gain,
):
    row_count, head_count, head_dim = queries_nope.shape
    rope_dim = queries_rope.shape[2]
    first_row = lax.axis_index("sp") * row_count
    query_turned = rotate(queries_rope.astype(jnp.float32), first_row).astype(jnp.bfloat16)
    key_turned = rotate(rope_key.astype(jnp.float32), first_row).astype(jnp.bfloat16)
    normed = latent_norm(latent, latent_gain)
    scale = (head_dim + rope_dim) ** (-0.5)
    query_places = first_row + jnp.arange(row_count, dtype=jnp.int32)
    last_place = first_row + row_count - 1

    def add_piece(carry, piece):
        top, denominators, weighted = carry
        latent_piece, rotary_piece = piece
        count = latent_piece.shape[0]
        keys = jnp.dot(latent_piece, key_up, preferred_element_type=jnp.float32).astype(
            jnp.bfloat16
        )
        keys = keys.reshape(count, head_count, head_dim)
        values_here = jnp.dot(latent_piece, value_up, preferred_element_type=jnp.float32).astype(
            jnp.bfloat16
        )
        values_here = values_here.reshape(count, head_count, head_dim)
        score = jnp.einsum("thd,shd->hts", queries_nope, keys, preferred_element_type=jnp.float32)
        score = score + jnp.einsum(
            "thr,sr->hts", query_turned, rotary_piece, preferred_element_type=jnp.float32
        )
        score = score * scale
        allowed = jnp.arange(count, dtype=jnp.int32)[None, :] <= query_places[:, None]
        score = jnp.where(allowed[None], score, big_negative)
        new_top = jnp.maximum(top, jnp.max(score, axis=2))
        powers = jnp.exp(score - new_top[:, :, None]) * allowed[None]
        shrink = jnp.exp(top - new_top)
        denominators = jnp.sum(powers, axis=2)
        weighted = weighted * shrink.T[:, :, None] + jnp.einsum(
            "hts,shd->thd",
            powers.astype(jnp.bfloat16),
            values_here,
            preferred_element_type=jnp.float32,
        )
        return (new_top, denominators, weighted)

    start_state = (
        jnp.full((head_count, row_count), big_negative, jnp.float32),
        jnp.zeros((head_count, row_count), jnp.float32),
        jnp.zeros((row_count, head_count, head_dim), jnp.float32),
    )
    piece = (
        lax.all_gather(normed, "sp", axis=0, tiled=True),
        lax.all_gather(key_turned, "sp", axis=0, tiled=True),
    )
    top, denominators, weighted = lax.cond(
        jnp.int32(0) <= last_place,
        lambda state: add_piece(state, piece),
        lambda state: state,
        start_state,
    )
    attended = (
        (weighted / denominators.T[:, :, None])
        .astype(jnp.bfloat16)
        .reshape(row_count, head_count * head_dim)
    )
    row_heads = lax.all_to_all(attended, "tp", split_axis=0, concat_axis=1, tiled=True)
    whole_proj = lax.all_gather(out_proj, "tp", axis=0, tiled=True)
    projected = jnp.dot(row_heads, whole_proj, preferred_element_type=jnp.float32)
    mixed = layer_norm(residual_weight * stream.astype(jnp.float32) + projected, mix_gain).astype(
        jnp.bfloat16
    )
    all_rows = lax.all_gather(mixed, "tp", axis=0, tiled=True)
    gate_sum = jnp.dot(
        all_rows,
        lax.all_gather(w_gate, "sp", axis=0, tiled=True),
        preferred_element_type=jnp.float32,
    )
    up_sum = jnp.dot(
        all_rows, lax.all_gather(w_up, "sp", axis=0, tiled=True), preferred_element_type=jnp.float32
    )
    hidden = (jax.nn.silu(gate_sum) * up_sum).astype(jnp.bfloat16)
    terms = jnp.dot(
        hidden, lax.all_gather(w_down, "sp", axis=1, tiled=True), preferred_element_type=jnp.float32
    )
    lowered = lax.psum_scatter(
        terms.astype(jnp.bfloat16), "tp", scatter_dimension=0, tiled=True
    ).astype(jnp.float32)
    return layer_norm(residual_weight * mixed.astype(jnp.float32) + 0.5 * lowered, mlp_gain).astype(
        jnp.bfloat16
    )


def solution(mesh):
    return jax.shard_map(
        per_device,
        mesh=mesh,
        in_specs=(
            P("sp", "tp", None),
            P("sp", "tp", None),
            P("sp", None),
            P("sp", None),
            P(),
            P(None, "tp"),
            P(None, "tp"),
            P("tp", None),
            P(("sp", "tp"), None),
            P(),
            P("sp", "tp"),
            P("sp", "tp"),
            P("tp", "sp"),
            P(),
        ),
        out_specs=P(("sp", "tp"), None),
        check_vma=False,
    )
```

profile of v0, /device:TPU:0, one launch (start us, length us, event | category | flops | bytes accessed | tf_op | source)
XLA Modules:
  0.0 365.5 jit_solution(3936866935383197673)
XLA Ops:
  6.5 0.0 copy-start.6
  6.5 0.0 copy-start.4
  6.5 0.0 copy-start.2
  6.5 0.0 all-gather.7.cloned.1.call-start
  6.5 1.2 fusion.19
  7.8 1.9 fusion.21
  9.7 0.0 all-gather.7.cloned.1.call-update
  9.7 0.0 all-gather.9.cloned.1.call-start
  9.7 0.7 all-gather.9.cloned.1.call-update
  10.5 0.0 all-gather.13.cloned.1.call-start
  10.5 0.7 all-gather.13.cloned.1.call-update
  11.2 0.0 all-gather.11.cloned.1.call-start
  11.2 0.8 convert_element_type.70
  12.0 0.0 copy-done.6
  12.1 0.3 multiply_cosine_fusion
  12.5 36.4 %all_gather.22 = bf16[3072,64]{0,1:T(8,128)(2,1)} all-gather(bf16[384,64]{0,1:T(8,128)(2,1)S(1)} %pad_maximum_fusion.1), channel_id=1, replica_groups=mesh['sp'=8,'tp'=4] {'sp'}, dimensions={0}, use_global_device_ids=true | all-gather | bytes 442368 | tf_op jit(solution)/shard_map/all_gather | solution.py:102
  48.8 26.7 %all-gather.7.cloned.1.call-done = bf16[3072,512]{1,0:T(8,128)(2,1)} async-done(((bf16[384,512]{1,0:T(8,128)(2,1)}), bf16[3072,512]{1,0:T(8,128)(2,1)}) %all-gather.7.cloned.1.call-update) | async-done | bytes 3145744 | tf_op jit(solution)/shard_map/all_gather | solution.py:101
  75.5 0.0 copy-done.4
  75.5 0.0 copy-done.2
  75.5 12.4 %conditional.1 = (f32[2,384]{1,0:T(2,128)S(1)}, f32[384,2,128]{0,2,1:T(8,128)S(1)}) conditional(s32[]{:T(128)} %convert_element_type.67, () %tuple.13, (s32[]{:T(128)}, s32[384]{0:T(512)S(1)}, bf16[3072,512]{1,0:T(8,128)(2,1)}, bf16[512,256]{1,0:T(8,128)(2,1)S(1)}, bf16[384,2,128]{2,1,0:T(2,128)(2,1)S(1)}, /*index=5*/bf16[3072,64]{0,1:T(8,128)(2,1)}, ...), branch_computations={%region_1.0_spmd, %region_2.5_spmd} | conditional | flops 3148186624 | bytes 93123176 | solution.py:104
  75.5 2.9 convolution_convert_fusion.1
  78.5 1.6 fusion.15
  80.0 0.0 copy-start.1
  80.0 1.0 fusion.17
  81.0 0.0 copy-done.1
  81.0 0.0 copy-start
  81.0 0.0 copy-start.3
  81.1 2.4 fusion.25
  83.5 0.0 copy-done
  83.5 0.0 copy-done.3
  83.5 1.1 convolution_convert_fusion
  84.5 1.9 fusion.11
  86.4 1.5 fusion.3
  88.0 0.2 copy.24
  88.2 0.1 all_to_all.14
  88.3 10.4 %all_to_all.19 = bf16[4,96,256]{2,1,0:T(8,128)(2,1)S(1)} all-to-all(bf16[4,96,256]{2,1,0:T(8,128)(2,1)S(1)} %all_to_all.14), channel_id=1, replica_groups=mesh['sp'=8,'tp'=4] {'tp'}, dimensions={0} | all-to-all | bytes 393216 | tf_op jit(solution)/shard_map/all_to_all | solution.py:115
  98.7 13.8 %all-gather.9.cloned.1.call-done = bf16[1024,2048]{1,0:T(8,128)(2,1)} async-done(((bf16[256,2048]{1,0:T(8,128)(2,1)}), bf16[1024,2048]{1,0:T(8,128)(2,1)}) %all-gather.9.cloned.1.call-update) | async-done | bytes 4194320 | tf_op jit(solution)/shard_map/all_gather | solution.py:116
  112.5 0.0 copy-start.5
  112.5 3.2 fusion.26
  115.7 0.2 multiply_reduce_fusion.1
  116.0 0.0 copy-done.5
  116.0 0.9 multiply_convert_fusion.1
  116.9 0.0 all-gather.11.cloned.1.call-update
  116.9 0.0 all-gather.15.cloned.1.call-start
  117.0 0.5 all-gather.15.cloned.1.call-update
  117.5 0.0 all-gather.17.cloned.1.call-start
  117.6 0.5 all-gather.17.cloned.1.call-update
  118.1 0.0 reduce-scatter.2.cloned.1.call-start
  118.1 56.6 %all-gather.13.cloned.1.call-done = bf16[2048,768]{1,0:T(8,128)(2,1)} async-done(((bf16[256,768]{1,0:T(8,128)(2,1)}), bf16[2048,768]{1,0:T(8,128)(2,1)}) %all-gather.13.cloned.1.call-update) | async-done | bytes 3145744 | tf_op jit(solution)/shard_map/all_gather | solution.py:124
  174.8 19.7 %all-gather.11.cloned.1.call-done = bf16[384,2048]{1,0:T(8,128)(2,1)} async-done(((bf16[96,2048]{1,0:T(8,128)(2,1)}), bf16[384,2048]{1,0:T(8,128)(2,1)}) %all-gather.11.cloned.1.call-update) | async-done | bytes 1572880 | tf_op jit(solution)/shard_map/all_gather | solution.py:121
  194.5 0.0 copy-start.8
  194.5 4.9 %fusion.27 = f32[384,768]{1,0:T(8,128)} fusion(bf16[384,2048]{1,0:T(8,128)(2,1)} %all-gather.11.cloned.1.call-done, bf16[2048,768]{1,0:T(8,128)(2,1)} %all-gather.13.cloned.1.call-done), kind=kOutput, calls=%fused_computation.56 | convolution fusion | flops 1207959552 | bytes 5898240 | tf_op jit(solution)/shard_map/dot_general | solution.py:122
  199.4 57.2 %all-gather.15.cloned.1.call-done = bf16[2048,768]{1,0:T(8,128)(2,1)} async-done(((bf16[256,768]{1,0:T(8,128)(2,1)}), bf16[2048,768]{1,0:T(8,128)(2,1)}) %all-gather.15.cloned.1.call-update) | async-done | bytes 3145744 | tf_op jit(solution)/shard_map/all_gather | solution.py:128
  256.6 63.2 %all-gather.17.cloned.1.call-done = bf16[768,2048]{1,0:T(8,128)(2,1)} async-done(((bf16[768,256]{1,0:T(8,128)(2,1)}), bf16[768,2048]{1,0:T(8,128)(2,1)}) %all-gather.17.cloned.1.call-update) | async-done | bytes 3145744 | tf_op jit(solution)/shard_map/all_gather | solution.py:132
  319.8 0.0 copy-done.8
  319.8 7.5 %convolution_convert_fusion.2 = bf16[384,2048]{1,0:T(8,128)(2,1)} fusion(bf16[768,2048]{1,0:T(8,128)(2,1)} %all-gather.17.cloned.1.call-done, bf16[384,2048]{1,0:T(8,128)(2,1)S(1)} %copy-done.8, bf16[2048,768]{1,0:T(8,128)(2,1)} %all-gather.15.cloned.1.call-done, f32[384,768]{1,0:T(8,128)} %fusion.27), kind=kOutput, calls=%fused_computation.21 | convolution fusion | flops 2418475008 | bytes 10616832 | tf_op jit(solution)/shard_map/dot_general | solution.py:131
  327.3 0.0 copy-start.7
  327.3 0.0 reduce-scatter.2.cloned.1.call-update
  327.3 26.3 %reduce-scatter.2.cloned.1.call-done = bf16[96,2048]{1,0:T(8,128)(2,1)} async-done(((bf16[384,2048]{1,0:T(8,128)(2,1)}), bf16[96,2048]{1,0:T(8,128)(2,1)}) %reduce-scatter.2.cloned.1.call-update) | async-done | bytes 393232 | tf_op jit(solution)/shard_map/reduce_scatter | solution.py:134
  353.6 1.4 fusion.23
  355.0 1.4 multiply_reduce_fusion
  356.5 0.0 copy-done.7
  356.5 2.2 multiply_convert_fusion
  (16 shorter events, 0.2 us)
Async XLA Ops:
  6.5 5.5 %copy-start.6 = (bf16[384,2,64]{0,2,1:T(8,128)(2,1)S(1)}, bf16[384,2,64]{0,2,1:T(8,128)(2,1)}, u32[]{:S(2)}) copy-start(bf16[384,2,64]{0,2,1:T(8,128)(2,1)} %param.17) | copy-start | bytes 294916
  6.5 69.0 %copy-start.4 = (bf16[384,2,128]{2,1,0:T(2,128)(2,1)S(1)}, bf16[384,2,128]{2,1,0:T(2,128)(2,1)}, u32[]{:S(2)}) copy-start(bf16[384,2,128]{2,1,0:T(2,128)(2,1)} %param.16) | copy-start | bytes 589828
  6.5 69.0 %copy-start.2 = (bf16[512,256]{1,0:T(8,128)(2,1)S(1)}, bf16[512,256]{1,0:T(8,128)(2,1)}, u32[]{:S(2)}) copy-start(bf16[512,256]{1,0:T(8,128)(2,1)} %param.21) | copy-start | bytes 786436
  6.5 69.0 %all-gather.7.cloned.1.call-start = ((), (), s32[]{:S(2)}) async-start(), calls=%async_computation.2 | async-start | bytes 3538944 | tf_op jit(solution)/shard_map/all_gather | solution.py:101
  9.7 102.8 %all-gather.9.cloned.1.call-start = ((), (), s32[]{:S(2)}) async-start(), calls=%async_computation.3 | async-start | bytes 5242880 | tf_op jit(solution)/shard_map/all_gather | solution.py:116
  10.5 164.3 %all-gather.13.cloned.1.call-start = ((), (), s32[]{:S(2)}) async-start(), calls=%async_computation.5 | async-start | bytes 3538944 | tf_op jit(solution)/shard_map/all_gather | solution.py:124
  11.2 183.3 %all-gather.11.cloned.1.call-start = ((), (), s32[]{:S(2)}) async-start(), calls=%async_computation.4 | async-start | bytes 1966080 | tf_op jit(solution)/shard_map/all_gather | solution.py:121
  80.0 1.0 copy-start.1
  81.0 2.4 copy-start
  81.0 2.4 copy-start.3
  112.5 3.5 copy-start.5
  116.9 139.6 %all-gather.15.cloned.1.call-start = ((), (), s32[]{:S(2)}) async-start(), calls=%async_computation.6 | async-start | bytes 3538944 | tf_op jit(solution)/shard_map/all_gather | solution.py:128
  117.5 202.3 %all-gather.17.cloned.1.call-start = ((), (), s32[]{:S(2)}) async-start(), calls=%async_computation.7 | async-start | bytes 3538944 | tf_op jit(solution)/shard_map/all_gather | solution.py:132
  118.1 235.5 %reduce-scatter.2.cloned.1.call-start = ((), (), s32[]{:S(2)}) async-start(), calls=%async_computation.8 | async-start | bytes 1966080 | tf_op jit(solution)/shard_map/reduce_scatter | solution.py:134
  194.5 125.3 %copy-start.8 = (bf16[384,2048]{1,0:T(8,128)(2,1)S(1)}, bf16[384,2048]{1,0:T(8,128)(2,1)}, u32[]{:S(2)}) copy-start(bf16[384,2048]{1,0:T(8,128)(2,1)} %all-gather.11.cloned.1.call-done) | copy-start | bytes 4718596
  327.3 29.2 %copy-start.7 = (f32[2048]{0:T(1024)S(1)}, f32[2048]{0:T(1024)}, u32[]{:S(2)}) copy-start(f32[2048]{0:T(1024)} %param.29) | copy-start | bytes 24580
Sparse Core Ops, SparseCore 0:
  9.8 65.6 all-gather.6
  77.1 35.3 all-gather.8
  114.7 60.0 all-gather.12
  176.2 18.2 all-gather.10
  196.5 60.0 all-gather.14
  258.5 61.3 all-gather.16
  327.4 26.1 reduce-scatter.1
where the time goes:
time: 366 us
  waiting for transfers between devices  266 us (73%)
  blocking collectives  46.8 us (13%)
  matrix products  25.3 us (7%)
  between operations  13.6 us (4%)
  other arithmetic  13 us (4%)
    all_gather x1, waiting for transfers between devices, per_device(): lax.all_gather(w_down, 'sp', axis=1, tiled=True)  63.2 us
    all_gather x1, waiting for transfers between devices, per_device(): lax.all_gather(w_up, 'sp', axis=0, tiled=True)  57.2 us
    all_gather x1, waiting for transfers between devices, per_device(): lax.all_gather(w_gate, 'sp', axis=0, tiled=True)  56.6 us
    all_gather x1, blocking collectives, per_device(): lax.all_gather(key_turned, 'sp', axis=0, tiled=True)  36.4 us
    all_gather x1, waiting for transfers between devices, per_device(): lax.all_gather(normed, 'sp', axis=0, tiled=True)  26.7 us
    reduce_scatter x1, waiting for transfers between devices, per_device(): lax.psum_scatter(terms.astype(jnp.bfloat16), 'tp', scatter_dimension=0, t...  26.3 us
    all_gather x1, waiting for transfers between devices, per_device(): all_rows = lax.all_gather(mixed, 'tp', axis=0, tiled=True)  19.7 us
    all_gather x1, waiting for transfers between devices, per_device(): whole_proj = lax.all_gather(out_proj, 'tp', axis=0, tiled=True)  13.8 us
  transfers between devices with their start and end apart: 7, of which 7 were waited for; matrix products, arithmetic and copies ran while one was open for 6% of the time, Pallas kernels for 0%

commit v1 on v0

--- a/solution.py
+++ b/solution.py
@@ -118,7 +118,12 @@
     mixed = layer_norm(residual_weight * stream.astype(jnp.float32) + projected, mix_gain).astype(
         jnp.bfloat16
     )
-    all_rows = lax.all_gather(mixed, "tp", axis=0, tiled=True)
+    ring = [mixed]
+    for hop in range(3):
+        ring.append(lax.ppermute(ring[-1], "tp", [(dev, (dev + 1) % 4) for dev in range(4)]))
+    all_rows = jnp.roll(
+        jnp.concatenate(ring[::-1], axis=0), (lax.axis_index("tp") + 1) * ring[0].shape[0], axis=0
+    )
     gate_sum = jnp.dot(
         all_rows,
         lax.all_gather(w_gate, "sp", axis=0, tiled=True),

time: 366 us -> 345 us (0.943)
  waiting for transfers between devices: 266 us -> 247 us
  blocking collectives: 46.8 us -> 36.5 us
  local copies, waits for them, and re-layouts: 0.35 us -> 5.72 us
  starting transfers between devices: 0.24 us -> 4.07 us
    all_gather x1, waiting for transfers between devices: 57.2 us -> 30.4 us  [per_device(): lax.all_gather(w_up, 'sp', axis=0, tiled=True)]
    ppermute x0 -> x3, waiting for transfers between devices: none -> 21.4 us  [per_device(): lax.ppermute(ring[-1], 'tp', [(dev, (dev + 1) % 4) for dev in range(4)])]
    all_gather x1 -> x0, waiting for transfers between devices: 19.7 us -> none  [per_device(): all_rows = lax.all_gather(mixed, 'tp', axis=0, tiled=True)]
    all_to_all x1 -> x0, blocking collectives: 10.4 us -> none  [per_device(): lax.all_to_all(attended, 'tp', split_axis=0, concat_axis=1, tiled=True)]
    all_to_all x0 -> x1, waiting for transfers between devices: none -> 6.98 us  [per_device(): lax.all_to_all(attended, 'tp', split_axis=0, concat_axis=1, tiled=True)]
    unnamed x12 -> x18, local copies, waits for them, and re-layouts: 0.02 us -> 4.71 us
  transfers between devices with their start and end apart: 7 -> 10, of which waited for: 7 -> 10; matrix products, arithmetic and copies ran while one was open for 6% -> 8% of each run, Pallas kernels for 0% -> 0%
where the time goes in v1:
time: 345 us
  waiting for transfers between devices  247 us (72%)
  blocking collectives  36.5 us (11%)
  matrix products  24.4 us (7%)
  between operations  13.7 us (4%)
  other arithmetic  13.4 us (4%)
  local copies, waits for them, and re-layouts  5.72 us (2%)
  starting transfers between devices  4.07 us (1%)
    all_gather x1, waiting for transfers between devices, per_device(): lax.all_gather(w_down, 'sp', axis=1, tiled=True)  63.2 us
    all_gather x1, waiting for transfers between devices, per_device(): lax.all_gather(w_gate, 'sp', axis=0, tiled=True)  57 us
    all_gather x1, blocking collectives, per_device(): lax.all_gather(key_turned, 'sp', axis=0, tiled=True)  36.5 us
    all_gather x1, waiting for transfers between devices, per_device(): lax.all_gather(w_up, 'sp', axis=0, tiled=True)  30.4 us
    all_gather x1, waiting for transfers between devices, per_device(): lax.all_gather(normed, 'sp', axis=0, tiled=True)  26.8 us
    reduce_scatter x1, waiting for transfers between devices, per_device(): lax.psum_scatter(terms.astype(jnp.bfloat16), 'tp', scatter_dimension=0, t...  26.4 us
    ppermute x3, waiting for transfers between devices, per_device(): lax.ppermute(ring[-1], 'tp', [(dev, (dev + 1) % 4) for dev in range(4)])  21.4 us
    all_gather x1, waiting for transfers between devices, per_device(): whole_proj = lax.all_gather(out_proj, 'tp', axis=0, tiled=True)  12.3 us
  transfers between devices with their start and end apart: 10, of which 10 were waited for; matrix products, arithmetic and copies ran while one was open for 8% of the time, Pallas kernels for 0%

profile of v1, /device:TPU:0, one launch (start us, length us, event | category | flops | bytes accessed | tf_op | source)
XLA Modules:
  0.0 344.7 jit_solution(17649478905595906989)
XLA Ops:
  6.5 0.0 all-gather.6.cloned.1.call-start
  6.6 1.2 fusion.22
  7.8 1.9 fusion.24
  9.7 0.0 all-gather.6.cloned.1.call-update
  9.8 0.0 all-gather.8.cloned.1.call-start
  9.8 0.7 all-gather.8.cloned.1.call-update
  10.5 0.0 all-gather.12.cloned.1.call-start
  10.6 0.7 all-gather.12.cloned.1.call-update
  11.2 0.0 all-gather.10.cloned.1.call-start
  11.3 0.5 all-gather.10.cloned.1.call-update
  11.8 0.0 copy-done.7
  11.9 0.0 copy-done.6
  11.9 0.3 multiply_cosine_fusion
  12.3 36.5 %all_gather.19 = bf16[3072,64]{0,1:T(8,128)(2,1)} all-gather(bf16[384,64]{0,1:T(8,128)(2,1)S(1)} %pad_maximum_fusion.1), channel_id=1, replica_groups=mesh['sp'=8,'tp'=4] {'sp'}, dimensions={0}, use_global_device_ids=true | all-gather | bytes 442368 | tf_op jit(solution)/shard_map/all_gather | solution.py:102
  48.7 26.8 %all-gather.6.cloned.1.call-done = bf16[3072,512]{1,0:T(8,128)(2,1)} async-done(((bf16[384,512]{1,0:T(8,128)(2,1)}), bf16[3072,512]{1,0:T(8,128)(2,1)}) %all-gather.6.cloned.1.call-update) | async-done | bytes 3145744 | tf_op jit(solution)/shard_map/all_gather | solution.py:101
  75.5 0.0 copy-done.5
  75.5 0.0 copy-done.3
  75.5 12.4 %conditional.1 = (f32[2,384]{1,0:T(2,128)S(1)}, f32[384,2,128]{0,2,1:T(8,128)S(1)}) conditional(s32[]{:T(128)} %convert_element_type.67, () %tuple.13, (s32[]{:T(128)}, s32[384]{0:T(512)S(1)}, bf16[3072,512]{1,0:T(8,128)(2,1)}, bf16[512,256]{1,0:T(8,128)(2,1)S(1)}, bf16[384,2,128]{2,1,0:T(2,128)(2,1)S(1)}, /*index=5*/bf16[3072,64]{0,1:T(8,128)(2,1)}, ...), branch_computations={%region_1.0_spmd, %region_2.5_spmd} | conditional | flops 3148186624 | bytes 93123176 | solution.py:104
  75.5 2.9 convolution_convert_fusion.1
  78.5 1.6 fusion.15
  80.0 0.0 copy-start.1
  80.0 1.0 fusion.17
  81.0 0.0 copy-done.1
  81.0 0.0 copy-start
  81.0 0.0 copy-start.4
  81.1 2.4 fusion.35
  83.5 1.0 convolution_convert_fusion
  84.5 1.9 fusion.11
  86.4 1.5 fusion.3
  88.0 0.2 copy.24
  88.2 0.8 all_to_all.14
  89.0 3.4 all-to-all-start
  92.4 0.0 all-gather.14.cloned.1.call-start
  92.4 0.5 all-gather.14.cloned.1.call-update
  93.0 0.2 reduce-scatter.2.cloned.1.call-start
  93.2 7.0 %all-to-all-done = bf16[4,96,256]{2,1,0:T(8,128)(2,1)S(1)} async-done(((bf16[4,96,256]{2,1,0:T(8,128)(2,1)}), bf16[4,96,256]{2,1,0:T(8,128)(2,1)S(1)}, u32[]{:S(2)}, u32[]{:S(2)}) %all-to-all-start) | async-done | bytes 196640 | tf_op jit(solution)/shard_map/all_to_all | solution.py:115
  100.2 12.3 %all-gather.8.cloned.1.call-done = bf16[1024,2048]{1,0:T(8,128)(2,1)} async-done(((bf16[256,2048]{1,0:T(8,128)(2,1)}), bf16[1024,2048]{1,0:T(8,128)(2,1)}) %all-gather.8.cloned.1.call-update) | async-done | bytes 4194320 | tf_op jit(solution)/shard_map/all_gather | solution.py:116
  112.5 3.2 fusion.36
  115.7 0.2 multiply_reduce_fusion.1
  116.0 0.2 multiply_convert_fusion.2
  116.2 0.3 collective-permute-start
  116.5 7.0 %collective-permute-done = bf16[96,2048]{1,0:T(8,128)(2,1)S(1)} collective-permute-done((bf16[96,2048]{1,0:T(8,128)(2,1)S(1)}, bf16[96,2048]{1,0:T(8,128)(2,1)S(1)}, u32[]{:S(2)}, u32[]{:S(2)}) %collective-permute-start) | collective-permute-done | bytes 393248 | tf_op jit(solution)/shard_map/ppermute | solution.py:123
  123.4 0.0 collective-permute-start.1
  123.4 7.2 %collective-permute-done.1 = bf16[96,2048]{1,0:T(8,128)(2,1)S(1)} collective-permute-done((bf16[96,2048]{1,0:T(8,128)(2,1)S(1)}, bf16[96,2048]{1,0:T(8,128)(2,1)S(1)}, u32[]{:S(2)}, u32[]{:S(2)}) %collective-permute-start.1) | collective-permute-done | bytes 393248 | tf_op jit(solution)/shard_map/ppermute | solution.py:123
  130.6 0.0 collective-permute-start.2
  130.6 7.2 %collective-permute-done.2 = bf16[96,2048]{1,0:T(8,128)(2,1)S(1)} collective-permute-done((bf16[96,2048]{1,0:T(8,128)(2,1)S(1)}, bf16[96,2048]{1,0:T(8,128)(2,1)S(1)}, u32[]{:S(2)}, u32[]{:S(2)}) %collective-permute-start.2) | collective-permute-done | bytes 393248 | tf_op jit(solution)/shard_map/ppermute | solution.py:123
  137.8 0.8 constant_dynamic-update-slice_fusion.7
  138.6 0.8 constant_dynamic-update-slice_fusion.6
  139.4 0.8 constant_dynamic-update-slice_fusion.5
  140.2 0.9 constant_dynamic-update-slice_fusion.4
  141.1 0.8 constant_dynamic-update-slice_fusion.3
  141.9 0.8 constant_dynamic-update-slice_fusion.2
  142.7 0.8 constant_dynamic-update-slice_fusion.1
  143.4 0.9 constant_dynamic-update-slice_fusion
  144.4 30.4 %all-gather.12.cloned.1.call-done = bf16[2048,768]{1,0:T(8,128)(2,1)} async-done(((bf16[256,768]{1,0:T(8,128)(2,1)}), bf16[2048,768]{1,0:T(8,128)(2,1)}) %all-gather.12.cloned.1.call-update) | async-done | bytes 3145744 | tf_op jit(solution)/shard_map/all_gather | solution.py:133
  174.8 3.8 %fusion.18 = f32[384,768]{1,0:T(8,128)S(1)} fusion(bf16[2048,768]{1,0:T(8,128)(2,1)} %all-gather.12.cloned.1.call-done, bf16[768,2048]{1,0:T(8,128)(2,1)} %constant_dynamic-update-slice_fusion, s32[]{:T(128)S(6)} %select_n.18), kind=kOutput, calls=%fused_computation.23 | convolution fusion | flops 1207959552 | bytes 5898244 | tf_op jit(solution)/shard_map/dot_general | solution.py:132
  178.5 57.0 %all-gather.10.cloned.1.call-done = bf16[2048,768]{1,0:T(8,128)(2,1)} async-done(((bf16[256,768]{1,0:T(8,128)(2,1)}), bf16[2048,768]{1,0:T(8,128)(2,1)}) %all-gather.10.cloned.1.call-update) | async-done | bytes 3145744 | tf_op jit(solution)/shard_map/all_gather | solution.py:129
  235.5 63.2 %all-gather.14.cloned.1.call-done = bf16[768,2048]{1,0:T(8,128)(2,1)} async-done(((bf16[768,256]{1,0:T(8,128)(2,1)}), bf16[768,2048]{1,0:T(8,128)(2,1)}) %all-gather.14.cloned.1.call-update) | async-done | bytes 3145744 | tf_op jit(solution)/shard_map/all_gather | solution.py:137
  298.7 7.6 %convolution_convert_fusion.2 = bf16[384,2048]{1,0:T(8,128)(2,1)} fusion(bf16[768,2048]{1,0:T(8,128)(2,1)} %all-gather.14.cloned.1.call-done, f32[384,768]{1,0:T(8,128)S(1)} %fusion.18, bf16[2048,768]{1,0:T(8,128)(2,1)} %all-gather.10.cloned.1.call-done, bf16[768,2048]{1,0:T(8,128)(2,1)} %constant_dynamic-update-slice_fusion, s32[]{:T(128)S(6)} %select_n.18), kind=kOutput, calls=%fused_computation.21 | convolution fusion | flops 2418475008 | bytes 10616836 | tf_op jit(solution)/shard_map/dot_general | solution.py:136
  306.4 0.0 reduce-scatter.2.cloned.1.call-update
  306.4 26.4 %reduce-scatter.2.cloned.1.call-done = bf16[96,2048]{1,0:T(8,128)(2,1)} async-done(((bf16[384,2048]{1,0:T(8,128)(2,1)}), bf16[96,2048]{1,0:T(8,128)(2,1)}) %reduce-scatter.2.cloned.1.call-update) | async-done | bytes 393232 | tf_op jit(solution)/shard_map/reduce_scatter | solution.py:139
  332.8 1.4 fusion.30
  334.2 1.4 multiply_reduce_fusion
  335.6 2.2 multiply_convert_fusion.1
  (27 shorter events, 0.2 us)
Async XLA Ops:
  6.5 5.3 %copy-start.7 = (bf16[384,64]{0,1:T(8,128)(2,1)S(1)}, bf16[384,64]{0,1:T(8,128)(2,1)}, u32[]{:S(2)}) copy-start(bf16[384,64]{0,1:T(8,128)(2,1)} %param.19) | copy-start | bytes 147460
  6.5 5.3 %copy-start.6 = (bf16[384,2,64]{0,2,1:T(8,128)(2,1)S(1)}, bf16[384,2,64]{0,2,1:T(8,128)(2,1)}, u32[]{:S(2)}) copy-start(bf16[384,2,64]{0,2,1:T(8,128)(2,1)} %param.17) | copy-start | bytes 294916
  6.5 69.0 %copy-start.5 = (bf16[384,2,128]{2,1,0:T(2,128)(2,1)S(1)}, bf16[384,2,128]{2,1,0:T(2,128)(2,1)}, u32[]{:S(2)}) copy-start(bf16[384,2,128]{2,1,0:T(2,128)(2,1)} %param.16) | copy-start | bytes 589828
  6.5 69.0 %copy-start.3 = (bf16[512,256]{1,0:T(8,128)(2,1)S(1)}, bf16[512,256]{1,0:T(8,128)(2,1)}, u32[]{:S(2)}) copy-start(bf16[512,256]{1,0:T(8,128)(2,1)} %param.21) | copy-start | bytes 786436
  6.5 69.0 %all-gather.6.cloned.1.call-start = ((), (), s32[]{:S(2)}) async-start(), calls=%async_computation.2 | async-start | bytes 3538944 | tf_op jit(solution)/shard_map/all_gather | solution.py:101
  9.8 102.8 %all-gather.8.cloned.1.call-start = ((), (), s32[]{:S(2)}) async-start(), calls=%async_computation.3 | async-start | bytes 5242880 | tf_op jit(solution)/shard_map/all_gather | solution.py:116
  10.5 164.2 %all-gather.12.cloned.1.call-start = ((), (), s32[]{:S(2)}) async-start(), calls=%async_computation.5 | async-start | bytes 3538944 | tf_op jit(solution)/shard_map/all_gather | solution.py:133
  11.2 224.3 %all-gather.10.cloned.1.call-start = ((), (), s32[]{:S(2)}) async-start(), calls=%async_computation.4 | async-start | bytes 3538944 | tf_op jit(solution)/shard_map/all_gather | solution.py:129
  80.0 1.0 copy-start.1
  81.0 2.4 copy-start
  81.0 2.4 copy-start.4
  89.0 11.2 %all-to-all-start = ((bf16[4,96,256]{2,1,0:T(8,128)(2,1)}), bf16[4,96,256]{2,1,0:T(8,128)(2,1)S(1)}, u32[]{:S(2)}, u32[]{:S(2)}) async-start(bf16[4,96,256]{2,1,0:T(8,128)(2,1)} %all_to_all.14), calls=%async_computation | async-start | bytes 393216 | tf_op jit(solution)/shard_map/all_to_all | solution.py:115
  92.4 206.4 %all-gather.14.cloned.1.call-start = ((), (), s32[]{:S(2)}) async-start(), calls=%async_computation.6 | async-start | bytes 3538944 | tf_op jit(solution)/shard_map/all_gather | solution.py:137
  93.0 239.8 %reduce-scatter.2.cloned.1.call-start = ((), (), s32[]{:S(2)}) async-start(), calls=%async_computation.7 | async-start | bytes 1966080 | tf_op jit(solution)/shard_map/reduce_scatter | solution.py:139
  112.5 3.5 %copy-start.2 = (f32[2048]{0:T(1024)S(1)}, f32[2048]{0:T(1024)}, u32[]{:S(2)}) copy-start(f32[2048]{0:T(1024)} %param.25) | copy-start | bytes 24580
  116.2 7.3 %collective-permute-start = (bf16[96,2048]{1,0:T(8,128)(2,1)S(1)}, bf16[96,2048]{1,0:T(8,128)(2,1)S(1)}, u32[]{:S(2)}, u32[]{:S(2)}) collective-permute-start(bf16[96,2048]{1,0:T(8,128)(2,1)S(1)} %multiply_convert_fusion.2), channel_id=1, source_target_pairs={{0,1},{1,2},{2,3},{3,0},{4,5},{5,6},{6,7},{7,4},{8,9},{9,10},{10,1... | collective-permute-start | bytes 1179656 | tf_op jit(solution)/shard_map/ppermute | solution.py:123
  123.4 7.2 %collective-permute-start.1 = (bf16[96,2048]{1,0:T(8,128)(2,1)S(1)}, bf16[96,2048]{1,0:T(8,128)(2,1)S(1)}, u32[]{:S(2)}, u32[]{:S(2)}) collective-permute-start(bf16[96,2048]{1,0:T(8,128)(2,1)S(1)} %collective-permute-done), channel_id=1, source_target_pairs={{0,1},{1,2},{2,3},{3,0},{4,5},{5,6},{6,7},{7,4},{8,9},{9,10},{10,1... | collective-permute-start | bytes 1179656 | tf_op jit(solution)/shard_map/ppermute | solution.py:123
  130.6 7.2 %collective-permute-start.2 = (bf16[96,2048]{1,0:T(8,128)(2,1)S(1)}, bf16[96,2048]{1,0:T(8,128)(2,1)S(1)}, u32[]{:S(2)}, u32[]{:S(2)}) collective-permute-start(bf16[96,2048]{1,0:T(8,128)(2,1)S(1)} %collective-permute-done.1), channel_id=1, source_target_pairs={{0,1},{1,2},{2,3},{3,0},{4,5},{5,6},{6,7},{7,4},{8,9},{9,10},{10,1... | collective-permute-start | bytes 1179656 | tf_op jit(solution)/shard_map/ppermute | solution.py:123
  306.4 29.3 %copy-start.8 = (f32[2048]{0:T(1024)S(1)}, f32[2048]{0:T(1024)}, u32[]{:S(2)}) copy-start(f32[2048]{0:T(1024)} %param.29) | copy-start | bytes 24580
Sparse Core Ops, SparseCore 0:
  9.9 65.6 all-gather.5
  77.1 35.3 all-gather.7
  114.7 60.0 all-gather.11
  176.8 58.6 all-gather.9
  237.4 61.2 all-gather.13
  306.5 26.2 reduce-scatter.1
